TPU v7x, 32 devices: a whole 2x2x4 slice. The times are simulated.
32 devices in a mesh: ep: 8 (over z, y), tp: 4 (over x, core).
Axes of the slice: x: 2, y: 2, z: 4, core: 2. Of those that a mesh axis runs over, the one named last changes fastest.
Arguments:
- mixer_in: bfloat16 [8192, 4096], P('ep', 'tp'), may hold values from -110 to 110
- mixer_gain: float32 [4096], P('tp'), may hold values from 0.1 to 1.9
- pool_weight: bfloat16 [4, 1024, 1024], P('tp'), may hold values from -0.1875 to 0.1875
- pool_scale: float32 [4096], P('tp'), may hold values from 0.1 to 1.9
- moe_in: bfloat16 [2048, 4096], P('ep'), may hold values from -6 to 6
- moe_gain: float32 [4096], replicated, may hold values from 0.1 to 1.9
- route_expert: int32 [2048, 2], P('ep'), may hold values from 0 to 7, as said below
- route_weight: float32 [2048, 2], P('ep'), may hold values from 0.1 to 1
- gate_weight: bfloat16 [8, 4096, 1024], P('ep', None, 'tp'), may hold values from -0.09375 to 0.09375
- up_weight: bfloat16 [8, 4096, 1024], P('ep', None, 'tp'), may hold values from -0.09375 to 0.09375
- down_weight: bfloat16 [8, 1024, 4096], P('ep', 'tp'), may hold values from -0.1875 to 0.1875
Outputs:
- mixer_out: bfloat16 [8192, 4096], P('ep', 'tp')
- moe_out: bfloat16 [2048, 4096], P('ep', 'tp')
Inputs may be any that keep to these rules, and one draw needn't show every extreme that they name: `route_expert`: both experts of a row are different and lie in one group: the group of an expert is its number divided by 2, rounded down. Among the rows of one index of ep no expert is named more than 96 times; in every draw the experts of some group are each named exactly 96 times by the rows of every index of ep.
All inputs are finite; a program needn't handle non-finite values.
Results may differ from a plain program's by a relative error of at most 0.0071.
Values may be sent and summed in bfloat16 or wider, within the bound.
No kernel may reach another device: no remote copies, remote signals or barrier semaphores. Data moves between devices by JAX's collectives and lax.ppermute only.
A program may use at most 128 MiB of HBM per device.

v0:
```python
import jax
import jax.numpy as jnp
from jax import lax
from jax.sharding import PartitionSpec as P

D = 4096
WINDOW_MAX = 16


EPS = 1e-06


def passed_along(value, axis, steps):
    count = lax.axis_size(axis)
    first, last = (max(0, -steps), min(count, count - steps))
    return lax.ppermute(value, axis, [(source, source + steps) for source in range(first, last)])


def shards(
    mixer_in,
    mixer_gain,
    pool_weight,
    pool_scale,
    moe_in,
    moe_gain,
    route_expert,
    route_weight,
    gate_weight,
    up_weight,
    down_weight,
):
    rows = mixer_in.shape[0]
    feats = mixer_in.astype(jnp.float32)
    squares = lax.psum(jnp.sum(feats * feats, axis=1), "tp")
    normed_a = (feats * lax.rsqrt(squares[:, None] / D + EPS) * mixer_gain).astype(jnp.bfloat16)
    reach = WINDOW_MAX - 1
    before = passed_along(normed_a[rows - reach :], "ep", 1)
    extended = jnp.concatenate([before, normed_a], axis=0).astype(jnp.float32)
    running = jnp.zeros((rows, normed_a.shape[1]), jnp.float32)
    totals = []
    for offset in range(WINDOW_MAX):
        running = running + lax.slice_in_dim(
            extended, reach - offset, reach - offset + rows, axis=0
        )
        if offset > 0 and offset + 1 & offset == 0:
            totals.append(running)
    group = lax.axis_index("tp")
    window_sum = lax.dynamic_index_in_dim(jnp.stack(totals), group, 0, keepdims=False)
    span = jnp.left_shift(jnp.int32(2), group)
    position = lax.axis_index("ep") * rows + jnp.arange(rows, dtype=jnp.int32)
    count = jnp.minimum(position + 1, span).astype(jnp.float32)[:, None]
    pooled = (window_sum / count - extended[reach:]).astype(jnp.bfloat16)
    mixer_out = (
        jnp.dot(pooled, pool_weight[0], preferred_element_type=jnp.float32) * pool_scale
    ).astype(jnp.bfloat16)
    tokens = moe_in.shape[0]
    feats_b = moe_in.astype(jnp.float32)
    normed_b = (
        feats_b * lax.rsqrt(jnp.mean(feats_b * feats_b, axis=1, keepdims=True) + EPS) * moe_gain
    ).astype(jnp.bfloat16)
    experts = gate_weight.shape[0] * lax.axis_size("ep")
    slots = 3 * tokens // experts
    flat = route_expert.reshape(-1)
    onehot = (flat[:, None] == jnp.arange(experts, dtype=jnp.int32)[None, :]).astype(jnp.int32)
    earlier = jnp.cumsum(onehot, axis=0) - onehot
    slot_index = flat * slots + jnp.sum(earlier * onehot, axis=1)
    owner = jnp.arange(2 * tokens, dtype=jnp.int32) // 2
    source = jnp.full((experts * slots,), tokens, jnp.int32).at[slot_index].set(owner)
    padded_b = jnp.concatenate([normed_b, jnp.zeros((1, D), jnp.bfloat16)], axis=0)
    outgoing = jnp.take(padded_b, source, axis=0).reshape(experts, slots, D)
    w_gate = gate_weight[0]
    w_up = up_weight[0]
    share = slots // lax.axis_size("tp")
    mine = lax.dynamic_slice_in_dim(outgoing, lax.axis_index("tp") * share, share, 1)
    arrived = lax.all_to_all(mine, "ep", split_axis=0, concat_axis=0, tiled=True)
    expand_arrived = lax.all_gather(arrived, "tp", axis=1, tiled=True)
    gate = jnp.einsum("nkd,df->nkf", expand_arrived, w_gate, preferred_element_type=jnp.float32)
    upper = jnp.einsum("nkd,df->nkf", expand_arrived, w_up, preferred_element_type=jnp.float32)
    hidden = (jax.nn.silu(gate) * upper).astype(jnp.bfloat16)
    flat_hidden = hidden.reshape(-1, hidden.shape[2])
    w_down = down_weight[0]
    columns = D // lax.axis_size("tp")
    summed = lax.psum_scatter(
        lax.dot_general(
            w_down, flat_hidden, (((0,), (1,)), ((), ())), preferred_element_type=jnp.float32
        ),
        "tp",
        scatter_dimension=0,
        tiled=True,
    ).astype(jnp.bfloat16)
    back = lax.all_to_all(
        summed.reshape(columns, -1, slots), "ep", split_axis=1, concat_axis=1, tiled=True
    )
    picked = jnp.take(back.reshape(columns, experts * slots), slot_index, axis=1)
    weighted = picked.astype(jnp.float32).reshape(columns, tokens, 2) * route_weight[None, :, :]
    moe_out = jnp.sum(weighted, axis=2).T.astype(jnp.bfloat16)
    return (mixer_out, moe_out)


def solution(mesh):
    return jax.shard_map(
        shards,
        mesh=mesh,
        in_specs=(
            P("ep", "tp"),
            P("tp"),
            P("tp", None, None),
            P("tp"),
            P("ep", None),
            P(),
            P("ep", None),
            P("ep", None),
            P("ep", None, "tp"),
            P("ep", None, "tp"),
            P("ep", "tp", None),
        ),
        out_specs=(P("ep", "tp"), P("ep", "tp")),
        check_vma=False,
    )
```

profile of v0, /device:TPU:0, one launch (start us, length us, event | category | flops | bytes accessed | tf_op | source)
XLA Modules:
  0.0 301.1 jit_solution(9724632331461842355)
XLA Ops:
  11.0 2.4 scatter_custom_fusion
  13.5 2.1 fusion.3
  15.7 2.2 fusion.5
  17.9 1.6 concatenate.7
  19.4 13.9 %gather_fusion = bf16[768,4096]{1,0:T(8,128)(2,1)} fusion(bf16[257,4096]{1,0:T(8,128)(2,1)} %concatenate.7, s32[1024]{0:T(1024)S(1)} %pad_clamp_fusion.1), kind=kCustom, calls=%fused_computation | custom fusion | bytes 12585984 | tf_op jit(solution)/shard_map/jit(_take)/gather | solution.py:70
  33.4 1.8 dynamic-slice_select_fusion
  35.2 44.2 %all_to_all.10 = bf16[8,24,4096]{2,1,0:T(8,128)(2,1)} all-to-all(bf16[8,24,4096]{2,1,0:T(8,128)(2,1)S(1)} %dynamic-slice_select_fusion), channel_id=1, replica_groups=mesh['ep'=8,'tp'=4] {'ep'}, dimensions={0} | all-to-all | bytes 3145728 | tf_op jit(solution)/shard_map/all_to_all | solution.py:75
  79.6 45.3 %all-gather.2.cloned.1.call-done = bf16[8,96,4096]{2,1,0:T(8,128)(2,1)} async-done(((bf16[8,24,4096]{2,1,0:T(8,128)(2,1)}), bf16[8,96,4096]{2,1,0:T(8,128)(2,1)}) %all-gather.2.cloned.1.call-update) | async-done | bytes 6291472 | tf_op jit(solution)/shard_map/all_gather | solution.py:76
  124.9 5.3 %fusion.17 = f32[8,96,256]{2,1,0:T(8,128)S(1)} fusion(bf16[8,96,4096]{2,1,0:T(8,128)(2,1)} %all-gather.2.cloned.1.call-done, bf16[1,4096,256]{2,1,0:T(8,128)(2,1)} %param.19), kind=kOutput, calls=%fused_computation.46 | convolution fusion | flops 1610612736 | bytes 9175040 | tf_op jit(solution)/shard_map/nkd,df->nkf/dot_general | solution.py:77
  130.8 1.8 fusion.25
  132.6 6.4 %convolution_bitcast_fusion = f32[4096,768]{0,1:T(8,128)} fusion(bf16[768,256]{1,0:T(8,128)(2,1)S(1)} %bitcast.65, bf16[1,256,4096]{2,1,0:T(8,128)(2,1)S(1)} %copy-done), kind=kOutput, calls=%fused_computation.7 | convolution fusion | flops 1610612736 | bytes 15073280 | tf_op jit(solution)/shard_map/dot_general | solution.py:84
  139.0 1.6 copy-done.2
  141.1 5.9 %psum.7 = f32[1024]{0:T(1024)S(1)} all-reduce(f32[1024]{0:T(1024)S(1)} %fusion), channel_id=1, replica_groups=mesh['ep'=8,'tp'=4] {'tp'}, use_global_device_ids=true, to_apply=%region_1.0 | all-reduce | flops 1024 | bytes 8192 | tf_op jit(solution)/shard_map/psum | solution.py:34
  147.0 2.9 fusion.2
  149.9 3.5 %collective-permute-start = (bf16[15,1024]{1,0:T(8,128)(2,1)S(1)}, bf16[15,1024]{1,0:T(8,128)(2,1)S(1)}, u32[]{:S(2)}, u32[]{:S(2)}) collective-permute-start(bf16[15,1024]{1,0:T(8,128)(2,1)S(1)} %slice.81), channel_id=1, source_target_pairs={{0,4},{4,8},{8,12},{12,16},{16,20},{20,24},{24,28},{1,5},{5,9},{9,... | collective-permute-start | bytes 92168 | tf_op jit(solution)/shard_map/ppermute | solution.py:16
  155.0 2.6 maximum_convert_fusion
  157.6 78.7 %reduce-scatter.2.cloned.1.call-done = f32[1024,768]{0,1:T(8,128)} async-done(((f32[4096,768]{0,1:T(8,128)}), f32[1024,768]{0,1:T(8,128)}) %reduce-scatter.2.cloned.1.call-update) | async-done | bytes 3145744 | tf_op jit(solution)/shard_map/reduce_scatter | solution.py:83
  236.3 3.3 %convert_element_type.62 = bf16[1024,768]{0,1:T(8,128)(2,1)} convert(f32[1024,768]{0,1:T(8,128)} %reduce-scatter.2.cloned.1.call-done) | non-fusion elementwise | flops 786432 | bytes 4718592 | tf_op jit(solution)/shard_map/convert_element_type | solution.py:90
  239.6 5.6 %all-to-all-start.1 = ((bf16[1024,8,96]{0,2,1:T(8,128)(2,1)}), bf16[1024,8,96]{0,2,1:T(8,128)(2,1)}, u32[]{:S(2)}, u32[]{:S(2)}) async-start(bf16[1024,8,96]{0,2,1:T(8,128)(2,1)} %bitcast.18), calls=%async_computation.2 | async-start | bytes 3145728 | tf_op jit(solution)/shard_map/all_to_all | solution.py:91
  245.3 28.7 %fusion.12 = (f32[1,1024,1024]{2,1,0:T(8,128)S(1)}, f32[1024,1024]{1,0:T(8,128)}, f32[1024,1024]{1,0:T(8,128)}, f32[1,1024,1024]{2,1,0:T(8,128)}) fusion(f32[1039,1024]{1,0:T(8,128)} %maximum_convert_fusion), kind=kLoop, calls=%fused_computation.25 | loop fusion | flops 15728640 | bytes 83886080 | tf_op jit(solution)/shard_map/stack | solution.py:48
  274.1 6.5 %multiply_convert_fusion = bf16[1024,1024]{1,0:T(8,128)(2,1)} fusion(bf16[1,1024,1024]{2,1,0:T(8,128)(2,1)S(1)} %copy-done.8, f32[1024]{0:T(1024)S(1)} %copy-done.9, s32[]{:T(128)S(6)} %select_n.44, f32[1,1024,1024]{2,1,0:T(8,128)S(1)} %get-tuple-element.2, f32[1,1024,1024]{2,1,0:T(8,128)} %bitcast.61, f32[1,1024,1024]{2,1,0:T(8,128)} %bitcast.62, ...), kind=kOutput, calls=%fused_computation.40 | convolution fusion | flops 2155872256 | bytes 25174020 | tf_op jit(solution)/shard_map/dot_general | solution.py:54
  280.6 1.6 all-to-all-done.1
  282.2 4.5 %gather_fusion.1 = bf16[512,1024]{1,0:T(8,128)(2,1)S(1)} fusion(bf16[1024,768]{0,1:T(8,128)(2,1)} %bitcast.19, s32[1024]{0:T(1024)S(1)} %pad_clamp_fusion), kind=kCustom, calls=%fused_computation.1 | custom fusion | bytes 2099200 | tf_op jit(solution)/shard_map/jit(_take)/gather | solution.py:94
  288.0 6.3 %multiply_reduce_fusion = bf16[1024,256]{0,1:T(8,128)(2,1)} fusion(bf16[1024,256,2]{0,2,1:T(2,128)(2,1)} %gather.15, pred[256,2]{1,0:T(8,128)(4,1)S(1)} %copy.22, f32[256,2]{1,0:T(8,128)S(1)} %copy.24), kind=kLoop, calls=%fused_computation.49 | loop fusion | flops 1835008 | bytes 1575424 | tf_op jit(solution)/shard_map/reduce_sum | solution.py:96
  (60 shorter events, 7.9 us)
Async XLA Ops:
  7.2 125.4 %copy-start = (bf16[1,256,4096]{2,1,0:T(8,128)(2,1)S(1)}, bf16[1,256,4096]{2,1,0:T(8,128)(2,1)}, u32[]{:S(2)}) copy-start(bf16[1,256,4096]{2,1,0:T(8,128)(2,1)} %param.21) | copy-start | bytes 6291460
  7.2 117.8 %all-gather.2.cloned.1.call-start = ((), (), s32[]{:S(2)}) async-start(), calls=%async_computation.3 | async-start | bytes 7864320 | tf_op jit(solution)/shard_map/all_gather | solution.py:76
  79.4 156.9 %reduce-scatter.2.cloned.1.call-start = ((), (), s32[]{:S(2)}) async-start(), calls=%async_computation.4 | async-start | bytes 15728640 | tf_op jit(solution)/shard_map/reduce_scatter | solution.py:83
  124.9 5.4 %copy-start.6 = (bf16[8,96,4096]{2,1,0:T(8,128)(2,1)S(1)}, bf16[8,96,4096]{2,1,0:T(8,128)(2,1)}, u32[]{:S(2)}) copy-start(bf16[8,96,4096]{2,1,0:T(8,128)(2,1)} %all-gather.2.cloned.1.call-done) | copy-start | bytes 18874372
  124.9 5.8 %copy-start.7 = (bf16[1,4096,256]{2,1,0:T(8,128)(2,1)S(1)}, bf16[1,4096,256]{2,1,0:T(8,128)(2,1)}, u32[]{:S(2)}) copy-start(bf16[1,4096,256]{2,1,0:T(8,128)(2,1)} %param.20) | copy-start | bytes 6291460
  139.0 1.6 copy-start.2
  139.0 8.0 %copy-start.4 = (f32[1024]{0:T(1024)S(1)}, f32[1024]{0:T(1024)}, u32[]{:S(2)}) copy-start(f32[1024]{0:T(1024)} %param.12) | copy-start | bytes 12292
  140.6 13.1 %copy-start.3 = (s32[256,2]{0,1:T(2,128)S(1)}, s32[256,2]{0,1:T(2,128)}, u32[]{:S(2)}) copy-start(s32[256,2]{0,1:T(2,128)} %param.17) | copy-start | bytes 6148
  140.6 13.3 %copy-start.5 = (f32[256,2]{0,1:T(2,128)S(1)}, f32[256,2]{0,1:T(2,128)}, u32[]{:S(2)}) copy-start(f32[256,2]{0,1:T(2,128)} %param.18) | copy-start | bytes 6148
  149.9 5.1 %collective-permute-start = (bf16[15,1024]{1,0:T(8,128)(2,1)S(1)}, bf16[15,1024]{1,0:T(8,128)(2,1)S(1)}, u32[]{:S(2)}, u32[]{:S(2)}) collective-permute-start(bf16[15,1024]{1,0:T(8,128)(2,1)S(1)} %slice.81), channel_id=1, source_target_pairs={{0,4},{4,8},{8,12},{12,16},{16,20},{20,24},{24,28},{1,5},{5,9},{9,... | collective-permute-start | bytes 92168 | tf_op jit(solution)/shard_map/ppermute | solution.py:16
  239.6 34.4 %slice-start = ((s8[4259840]{0:T(1024)(128)(4,1)}), s8[65536]{0:T(1024)(128)(4,1)S(1)}, s32[]{:S(2)}) async-start(s8[4259840]{0:T(1024)(128)(4,1)} %bitcast.58), calls=%async_computation.5 | async-start | bytes 131072
  239.6 42.6 %all-to-all-start.1 = ((bf16[1024,8,96]{0,2,1:T(8,128)(2,1)}), bf16[1024,8,96]{0,2,1:T(8,128)(2,1)}, u32[]{:S(2)}, u32[]{:S(2)}) async-start(bf16[1024,8,96]{0,2,1:T(8,128)(2,1)} %bitcast.18), calls=%async_computation.2 | async-start | bytes 3145728 | tf_op jit(solution)/shard_map/all_to_all | solution.py:91
  245.3 28.8 %slice-start.1 = ((s8[4259840]{0:T(1024)(128)(4,1)}), s8[4194304]{0:T(1024)(128)(4,1)S(1)}, s32[]{:S(2)}) async-start(s8[4259840]{0:T(1024)(128)(4,1)} %bitcast.58), calls=%async_computation.6 | async-start | bytes 8388608
  245.3 28.8 %copy-start.8 = (bf16[1,1024,1024]{2,1,0:T(8,128)(2,1)S(1)}, bf16[1,1024,1024]{2,1,0:T(8,128)(2,1)}, u32[]{:S(2)}) copy-start(bf16[1,1024,1024]{2,1,0:T(8,128)(2,1)} %param.13) | copy-start | bytes 6291460
  245.3 28.8 %copy-start.9 = (f32[1024]{0:T(1024)S(1)}, f32[1024]{0:T(1024)}, u32[]{:S(2)}) copy-start(f32[1024]{0:T(1024)} %param.14) | copy-start | bytes 12292
  282.2 12.1 %copy-start.1 = (bf16[1,256,4096]{2,1,0:T(8,128)(2,1)S(1)}, bf16[1,256,4096]{2,1,0:T(8,128)(2,1)}, u32[]{:S(2)}) copy-start(bf16[1,256,4096]{2,1,0:T(8,128)(2,1)} %param.21) | copy-start | bytes 6291460
Sparse Core Ops, SparseCore 0:
  79.5 45.3 all-gather.1
  139.1 97.1 reduce-scatter.1
where the time goes:
time: 302 us; the launch traced here: 301 us
  waiting for transfers between devices  127 us (42%)
  other arithmetic  52.6 us (17%)
  blocking collectives  50.1 us (17%)
  local copies, waits for them, and re-layouts  27.9 us (9%)
  matrix products  20.1 us (7%)
  between operations  14.3 us (5%)
  starting transfers between devices  9.46 us (3%)
    reduce_scatter x1, waiting for transfers between devices, shards(): lax.psum_scatter(lax.dot_general(w_down, flat_hidden, (((0,), (1,)), ((),...  78.7 us
    all_gather x1, waiting for transfers between devices, shards(): expand_arrived = lax.all_gather(arrived, 'tp', axis=1, tiled=True)  45.3 us
    all_to_all x1, blocking collectives, shards(): lax.all_to_all(mine, 'ep', split_axis=0, concat_axis=0, tiled=True)  44.2 us
    another operation x1, other arithmetic, shards(): jnp.stack(totals)  28.7 us
    gather x1, local copies, waits for them, and re-layouts, shards(): outgoing = jnp.take(padded_b, source, axis=0).reshape(experts, slots, D)  13.9 us
    dot_general x1, matrix products, shards(): jnp.dot(pooled, pool_weight[0], preferred_element_type=jnp.float32)  6.54 us
    dot_general x1, matrix products, shards(): lax.dot_general(w_down, flat_hidden, (((0,), (1,)), ((), ())), preferred_...  6.38 us
    reduce_sum x1, other arithmetic, shards(): moe_out = jnp.sum(weighted, axis=2).T.astype(jnp.bfloat16)  6.33 us
  transfers between devices with their start and end apart: 4, of which 4 were waited for; matrix products, arithmetic and copies ran while one was open for 14% of the time, Pallas kernels for 0%

commit v1 on v0

--- a/solution.py
+++ b/solution.py
@@ -1,10 +1,13 @@
 import jax
 import jax.numpy as jnp
 from jax import lax
-from jax.sharding import PartitionSpec as P
+from jax.experimental import pallas as pl
+from jax.experimental.pallas import tpu as pltpu
+from jax.sharding import Mesh, PartitionSpec as P
 
 D = 4096
 WINDOW_MAX = 16
+EXPERT_GROUPS = 4
 
 
 EPS = 1e-06
@@ -97,23 +100,353 @@
     return (mixer_out, moe_out)
 
 
+F32, BF16, I32 = jnp.float32, jnp.bfloat16, jnp.int32
+EXTRA = 128
+
+
+def swapped(value, axis):
+    return lax.ppermute(value, axis, [(i, i ^ 1) for i in range(lax.axis_size(axis))])
+
+
+def turned(value, axis, steps):
+    count = lax.axis_size(axis)
+    return lax.ppermute(value, axis, [(i, (i + steps) % count) for i in range(count)])
+
+
+def vmem():
+    return pl.BlockSpec(memory_space=pltpu.VMEM)
+
+
+def smem():
+    return pl.BlockSpec(memory_space=pltpu.SMEM)
+
+
+def dot(a, b):
+    return jnp.dot(a, b, preferred_element_type=F32)
+
+
+def dispatch(moe_in, moe_gain, expert_rows, weight_rows, place, cap):
+    tokens, width = moe_in.shape
+    half = cap // 2
+    groups = EXPERT_GROUPS
+
+    def kernel(place_ref, x_ref, gain_ref, expert_ref, weight_ref, key_ref, *out_refs):
+        x = x_ref[...].astype(F32)
+        scale = lax.rsqrt(jnp.sum(x * x, axis=1, keepdims=True) / width + EPS)
+        normed = (x * scale * gain_ref[...]).astype(BF16)
+        z, c = place_ref[0], place_ref[1]
+        expert = expert_ref[...]
+        first = expert[0:1]
+        group = lax.shift_right_logical(first, 1)
+        member = (lax.broadcasted_iota(I32, (8, tokens), 0) == group).astype(F32)
+        before = lax.broadcasted_iota(I32, (tokens, tokens), 0) < lax.broadcasted_iota(
+            I32, (tokens, tokens), 1
+        )
+        earlier = dot(member.astype(BF16), before.astype(BF16))
+        slot = jnp.sum(member * earlier, axis=0, keepdims=True).astype(I32)
+        ahead = group - z
+        ahead = jnp.where(ahead < 0, ahead + groups, ahead)
+        local = slot - c * half
+        mine = (local >= 0) & (local < half)
+        local = jnp.where(local < 0, local + cap, local)
+        key_ref[...] = jnp.broadcast_to(ahead * cap + local, (8, tokens))
+        sent = jnp.where(mine, ahead * half + local, -1)
+        pick = (lax.broadcasted_iota(I32, (groups * half, tokens), 0) == sent).astype(BF16)
+        weight = weight_ref[...]
+        even = (first & 1) == 0
+        low = jnp.where(even, weight[0:1], weight[1:2])
+        high = jnp.where(even, weight[1:2], weight[0:1])
+        parts = []
+        for w in (low, high):
+            top = w.astype(BF16)
+            parts += [top, (w - top.astype(F32)).astype(BF16)]
+        lane = lax.broadcasted_iota(I32, (8, EXTRA), 1)
+        row = lax.broadcasted_iota(I32, (8, EXTRA), 0)
+        spread = (lane == row).astype(BF16)
+        stacked = jnp.concatenate(
+            [p.astype(F32) for p in parts] + [jnp.zeros((4, tokens), F32)], axis=0
+        ).astype(BF16)
+        table = lax.dot_general(
+            stacked, spread, (((0,), (0,)), ((), ())), preferred_element_type=F32
+        ).astype(BF16)
+        rows = dot(pick, normed).astype(BF16)
+        extra = dot(pick, table).astype(BF16)
+        for d in range(groups):
+            out_refs[d][:, :width] = rows[d * half : (d + 1) * half]
+            out_refs[d][:, width:] = extra[d * half : (d + 1) * half]
+
+    return pl.pallas_call(
+        kernel,
+        out_shape=[jax.ShapeDtypeStruct((8, tokens), I32)]
+        + [jax.ShapeDtypeStruct((half, width + EXTRA), BF16)] * groups,
+        in_specs=[smem(), vmem(), vmem(), vmem(), vmem()],
+        out_specs=[vmem()] * (1 + groups),
+        name="dispatch",
+    )(place, moe_in, moe_gain.reshape(1, width), expert_rows, weight_rows)
+
+
+def expand(pieces, w_gate, w_up, pair):
+    width, units = w_gate.shape
+    step = 512
+    steps = width // step
+    total = sum(p.shape[0] for p in pieces)
+    count = len(pieces)
+
+    def kernel(pair_ref, *refs):
+        xs, extras = refs[:count], refs[count : 2 * count]
+        gate_ref, up_ref, out_ref, gate_sum, up_sum = refs[2 * count :]
+        k = pl.program_id(0)
+
+        @pl.when(k == 0)
+        def _():
+            gate_sum[...] = jnp.zeros_like(gate_sum)
+            up_sum[...] = jnp.zeros_like(up_sum)
+
+        x = jnp.concatenate([r[...] for r in xs], axis=0)
+        gate_sum[...] += dot(x, gate_ref[...])
+        up_sum[...] += dot(x, up_ref[...])
+
+        @pl.when(k == steps - 1)
+        def _():
+            extra = jnp.concatenate([r[...] for r in extras], axis=0).astype(F32)
+            lane = lax.broadcasted_iota(I32, extra.shape, 1)
+            wanted = lax.shift_right_logical(lane, 1) == pair_ref[0]
+            weight = jnp.sum(jnp.where(wanted, extra, 0.0), axis=1, keepdims=True)
+            gate = gate_sum[...]
+            out_ref[...] = (gate / (1.0 + jnp.exp(-gate)) * up_sum[...] * weight).astype(BF16)
+
+    return pl.pallas_call(
+        kernel,
+        grid=(steps,),
+        out_shape=jax.ShapeDtypeStruct((total, units), BF16),
+        in_specs=[smem()]
+        + [pl.BlockSpec((p.shape[0], step), lambda k: (0, k)) for p in pieces]
+        + [pl.BlockSpec((p.shape[0], EXTRA), lambda k: (0, width // EXTRA)) for p in pieces]
+        + [pl.BlockSpec((step, units), lambda k: (k, 0))] * 2,
+        out_specs=pl.BlockSpec((total, units), lambda k: (0, 0)),
+        scratch_shapes=[pltpu.VMEM((total, units), F32)] * 2,
+        name="expand",
+    )(pair, *pieces, *pieces, w_gate, w_up)
+
+
+def contract(own, beside, across, w_own, w_beside, w_across, runs):
+    units = own.shape[1]
+    columns = w_own.shape[1]
+    kept = sum(n for _, n, other, _ in runs if not other)
+    total = own.shape[0]
+
+    def kernel(own_ref, beside_ref, across_ref, wo_ref, wb_ref, wa_ref, keep_ref, send_ref):
+        near = [s for s, _, _, far in runs if not far]
+        far = [s for s, _, _, far in runs if far]
+        partner = dict(zip(near + far, far + near))
+        swapped_rows = jnp.concatenate(
+            [across_ref[partner[s] : partner[s] + n] for s, n, _, _ in runs], axis=0
+        )
+        out = dot(own_ref[...], wo_ref[...])
+        out = out + dot(beside_ref[...], wb_ref[...])
+        out = out + dot(swapped_rows, wa_ref[...])
+        out = out.astype(BF16)
+        at = {False: 0, True: 0}
+        for s, n, other, _ in runs:
+            ref = send_ref if other else keep_ref
+            ref[at[other] : at[other] + n] = out[s : s + n]
+            at[other] += n
+
+    return pl.pallas_call(
+        kernel,
+        out_shape=[
+            jax.ShapeDtypeStruct((kept, columns), BF16),
+            jax.ShapeDtypeStruct((total - kept, columns), BF16),
+        ],
+        in_specs=[vmem()] * 6,
+        out_specs=[vmem()] * 2,
+        name="contract",
+    )(own, beside, across, w_own, w_beside, w_across)
+
+
+def restore(key, pieces):
+    tokens = key.shape[1]
+    cap, columns = pieces[0].shape
+
+    def kernel(key_ref, *refs):
+        out_ref = refs[-1]
+        total = None
+        for d, r in enumerate(refs[:-1]):
+            row = lax.broadcasted_iota(I32, (cap, tokens), 0) + d * cap
+            pick = (row == key_ref[0:1]).astype(BF16)
+            part = lax.dot_general(
+                pick, r[...], (((0,), (0,)), ((), ())), preferred_element_type=F32
+            )
+            total = part if total is None else total + part
+        out_ref[...] = total.astype(BF16)
+
+    return pl.pallas_call(
+        kernel,
+        out_shape=jax.ShapeDtypeStruct((tokens, columns), BF16),
+        in_specs=[vmem()] * (1 + len(pieces)),
+        out_specs=vmem(),
+        name="restore",
+    )(key, *pieces)
+
+
+def pool(mixer_in, halo, squares, gain, weight, scale, place):
+    rows, width = mixer_in.shape
+    reach = WINDOW_MAX
+    block = 256
+    steps = rows // block
+
+    def kernel(place_ref, x_ref, prev_ref, halo_ref, sq_ref, psq_ref, gain_ref, w_ref, s_ref, out_ref):
+        i = pl.program_id(0)
+        span = lax.shift_left(jnp.int32(2), place_ref[1])
+        ahead = jnp.where(i == 0, halo_ref[...].astype(F32), prev_ref[...].astype(F32))
+        x = jnp.concatenate([ahead, x_ref[...].astype(F32)], axis=0)
+        total = jnp.concatenate([psq_ref[...], sq_ref[...]], axis=0)
+        normed = (x * lax.rsqrt(total / D + EPS) * gain_ref[...]).astype(BF16)
+        r = lax.broadcasted_iota(I32, (block, block + reach), 0)
+        q = lax.broadcasted_iota(I32, (block, block + reach), 1)
+        back = r + reach - q
+        band = ((back >= 0) & (back < span)).astype(BF16)
+        sums = dot(band, normed)
+        position = place_ref[0] * rows + i * block + lax.broadcasted_iota(I32, (block, 1), 0)
+        count = jnp.minimum(position + 1, span).astype(F32)
+        pooled = (sums / count - normed[reach:].astype(F32)).astype(BF16)
+        out_ref[...] = (dot(pooled, w_ref[...]) * s_ref[...]).astype(BF16)
+
+    ratio = block // reach
+    return pl.pallas_call(
+        kernel,
+        grid=(steps,),
+        out_shape=jax.ShapeDtypeStruct((rows, width), BF16),
+        in_specs=[
+            smem(),
+            pl.BlockSpec((block, width), lambda i: (i, 0)),
+            pl.BlockSpec((reach, width), lambda i: (jnp.maximum(i * ratio - 1, 0), 0)),
+            pl.BlockSpec((reach, width), lambda i: (0, 0)),
+            pl.BlockSpec((block, 1), lambda i: (i, 0)),
+            pl.BlockSpec((reach, 1), lambda i: (jnp.where(i == 0, steps * ratio, i * ratio - 1), 0)),
+            pl.BlockSpec((1, width), lambda i: (0, 0)),
+            pl.BlockSpec((width, width), lambda i: (0, 0)),
+            pl.BlockSpec((1, width), lambda i: (0, 0)),
+        ],
+        out_specs=pl.BlockSpec((block, width), lambda i: (i, 0)),
+        name="pool",
+    )(
+        place,
+        mixer_in,
+        mixer_in,
+        halo,
+        squares,
+        squares,
+        gain.reshape(1, width),
+        weight,
+        scale.reshape(1, width),
+    )
+
+
+def paired(
+    mixer_in,
+    mixer_gain,
+    pool_weight,
+    pool_scale,
+    moe_in,
+    moe_gain,
+    route_expert,
+    route_weight,
+    gate_weight,
+    up_weight,
+    down_weight,
+):
+    z, y, x, c = (lax.axis_index(a) for a in ("z", "y", "x", "c"))
+    tokens = moe_in.shape[0]
+    cap = 3 * tokens // (2 * EXPERT_GROUPS)
+    half = cap // 2
+
+    key, *sends = dispatch(
+        moe_in, moe_gain, route_expert.T, route_weight.T, jnp.stack([z, c]).astype(I32), cap
+    )
+    come = [sends[0], turned(sends[1], "z", 1), turned(sends[2], "z", 2), turned(sends[3], "z", 3)]
+    other = [swapped(v, "y") for v in come]
+    w_gate, w_up, w_down = gate_weight[0], up_weight[0], down_weight[0]
+
+    quarter = w_down.shape[1] // (2 * lax.axis_size("x"))
+    away = lax.dynamic_slice_in_dim(w_down, (1 - x) * 2 * quarter, 2 * quarter, 1)
+    w_beside2 = swapped(away, "x")
+    mine_at, twin_at = (2 * x + c) * quarter, (2 * x + 1 - c) * quarter
+    w_own = lax.dynamic_slice_in_dim(w_down, mine_at, quarter, 1)
+    w_beside = lax.dynamic_slice_in_dim(w_beside2, c * quarter, quarter, 1)
+    w_across = swapped(
+        jnp.concatenate(
+            [
+                lax.dynamic_slice_in_dim(w_down, twin_at, quarter, 1),
+                lax.dynamic_slice_in_dim(w_beside2, (1 - c) * quarter, quarter, 1),
+            ],
+            axis=0,
+        ),
+        "c",
+    )
+
+    pair = y.astype(I32).reshape(1)
+    results = [None] * EXPERT_GROUPS
+    for chunk in ((0, 1, 3), (2,)):
+        near = [v for d in chunk for v in (come[d], other[d])]
+        far = [swapped(v, "c") for v in near]
+        hidden = expand(near + far, w_gate, w_up, pair)
+        beside = swapped(hidden, "x")
+        across = swapped(jnp.concatenate([hidden, beside], axis=1), "c")
+        runs = []
+        for is_far in (False, True):
+            for d in chunk:
+                for is_other in (False, True):
+                    runs.append((len(runs) * half, half, is_other, is_far))
+        keep, send = contract(hidden, beside, across, w_own, w_beside, w_across, runs)
+        got = swapped(send, "y")
+        both = (keep.astype(F32) + got.astype(F32)).astype(BF16)
+        n = len(chunk)
+        for at, d in enumerate(chunk):
+            rows = jnp.concatenate(
+                [both[at * half : (at + 1) * half], both[(n + at) * half : (n + at + 1) * half]], axis=0
+            )
+            results[d] = turned(rows, "z", -d) if d else rows
+    moe_out = restore(key, results)
+
+    rows = mixer_in.shape[0]
+    reach = WINDOW_MAX
+    halo = passed_along(mixer_in[rows - reach :], ("z", "y"), 1)
+    squares = jnp.concatenate(
+        [jnp.sum(jnp.square(v.astype(F32)), axis=1) for v in (mixer_in, halo)]
+    )
+    squares = squares + swapped(squares, "c")
+    squares = squares + swapped(squares, "x")
+    place = jnp.stack([z * lax.axis_size("y") + y, 2 * x + c]).astype(I32)
+    mixer_out = pool(
+        mixer_in, halo, squares[:, None], mixer_gain, pool_weight[0], pool_scale, place
+    )
+    return (mixer_out, moe_out)
+
+
 def solution(mesh):
+    ep, tp = mesh.shape["ep"], mesh.shape["tp"]
+    body, over, a, b = shards, mesh, "ep", "tp"
+    if ep == 2 * EXPERT_GROUPS and tp == 4:
+        shape = (EXPERT_GROUPS, 2, 2, 2)
+        over = Mesh(mesh.devices.reshape(shape), ("z", "y", "x", "c"))
+        body, a, b = paired, ("z", "y"), ("x", "c")
     return jax.shard_map(
-        shards,
-        mesh=mesh,
+        body,
+        mesh=over,
         in_specs=(
-            P("ep", "tp"),
-            P("tp"),
-            P("tp", None, None),
-            P("tp"),
-            P("ep", None),
+            P(a, b),
+            P(b),
+            P(b, None, None),
+            P(b),
+            P(a, None),
             P(),
-            P("ep", None),
-            P("ep", None),
-            P("ep", None, "tp"),
-            P("ep", None, "tp"),
-            P("ep", "tp", None),
+            P(a, None),
+            P(a, None),
+            P(a, None, b),
+            P(a, None, b),
+            P(a, b, None),
         ),
-        out_specs=(P("ep", "tp"), P("ep", "tp")),
+        out_specs=(P(a, b), P(a, b)),
         check_vma=False,
     )

time: 302 us -> 146 us (0.48)
  waiting for transfers between devices: 127 us -> 48.4 us
  blocking collectives: 50.1 us -> 0 us
  other arithmetic: 52.6 us -> 7.51 us
  Pallas kernels: 0 us -> 37.6 us
  starting transfers between devices: 9.46 us -> 38.6 us
  matrix products: 20.1 us -> 0 us
  local copies, waits for them, and re-layouts: 27.9 us -> 10.9 us
  between operations: 14.3 us -> 0.82 us
    reduce_scatter x1 -> x0, waiting for transfers between devices: 78.7 us -> none  [shards(): lax.psum_scatter(lax.dot_general(w_down, flat_hidden, (((0,), (1,)), ((),...]
    ppermute x0 -> x28, waiting for transfers between devices: none -> 48.4 us  [the longest x22 26.4 us: swapped(): lax.ppermute(value, axis, [(i, i ^ 1) for i in range(lax.axis_size(axis))])]
    all_gather x1 -> x0, waiting for transfers between devices: 45.3 us -> none  [shards(): expand_arrived = lax.all_gather(arrived, 'tp', axis=1, tiled=True)]
    all_to_all x1 -> x0, blocking collectives: 44.2 us -> none  [shards(): lax.all_to_all(mine, 'ep', split_axis=0, concat_axis=0, tiled=True)]
    pallas_call x0 -> x7, Pallas kernels: none -> 37.6 us  [the longest x2 16.2 us: expand(): pl.pallas_call(kernel, grid=(steps,), out_shape=jax.ShapeDtypeStruct((tot...]
    ppermute x0 -> x28, starting transfers between devices: none -> 35.6 us  [the longest x6 20.2 us: turned(): lax.ppermute(value, axis, [(i, (i + steps) % count) for i in range(count)])]
    another operation x3 -> x2, other arithmetic: 29.9 us -> 1.23 us  [the longest x1 0.65 us: paired(): jnp.stack([z, c]).astype(I32)]
    dot_general x4 -> x0, matrix products: 20.1 us -> none  [the longest x1 6.54 us: shards(): jnp.dot(pooled, pool_weight[0], preferred_element_type=jnp.float32)]
  transfers between devices with their start and end apart: 4 -> 29, of which waited for: 4 -> 8; matrix products, arithmetic and copies ran while one was open for 14% -> 8% of each run, Pallas kernels for 0% -> 24%
where the time goes in v1:
time: 146 us; the launch traced here: 144 us
  waiting for transfers between devices  48.4 us (33%)
  starting transfers between devices  38.6 us (26%)
  Pallas kernels  37.6 us (26%)
  local copies, waits for them, and re-layouts  10.9 us (7%)
  other arithmetic  7.51 us (5%)
    ppermute x22, waiting for transfers between devices, swapped(): lax.ppermute(value, axis, [(i, i ^ 1) for i in range(lax.axis_size(axis))])  26.4 us
    ppermute x6, waiting for transfers between devices, turned(): lax.ppermute(value, axis, [(i, (i + steps) % count) for i in range(count)])  21.9 us
    ppermute x6, starting transfers between devices, turned(): lax.ppermute(value, axis, [(i, (i + steps) % count) for i in range(count)])  20.2 us
    pallas_call x2, Pallas kernels, expand(): pl.pallas_call(kernel, grid=(steps,), out_shape=jax.ShapeDtypeStruct((tot...  16.2 us
    ppermute x22, starting transfers between devices, swapped(): lax.ppermute(value, axis, [(i, i ^ 1) for i in range(lax.axis_size(axis))])  15.4 us
    pallas_call x1, Pallas kernels, pool(): pl.pallas_call(kernel, grid=(steps,), out_shape=jax.ShapeDtypeStruct((row...  7.38 us
    pallas_call x2, Pallas kernels, contract(): pl.pallas_call(kernel, out_shape=[jax.ShapeDtypeStruct((kept, columns), B...  7.33 us
    pallas_call x1, Pallas kernels, dispatch(): pl.pallas_call(kernel, out_shape=[jax.ShapeDtypeStruct((8, tokens), I32)]...  3.95 us
  transfers between devices with their start and end apart: 29, of which 8 were waited for; matrix products, arithmetic and copies ran while one was open for 8% of the time, Pallas kernels for 24%

profile of v1, /device:TPU:0, one launch (start us, length us, event | category | flops | bytes accessed | tf_op | source)
XLA Modules:
  0.0 143.8 jit_solution(2273362882398862323)
XLA Ops:
  0.6 2.5 %dynamic-slice_bitcast_fusion = bf16[256,2048]{1,0:T(8,128)(2,1)} fusion(bf16[1,256,4096]{2,1,0:T(8,128)(2,1)} %param.21, s32[]{:T(128)S(6)} %select_n.16), kind=kLoop, calls=%fused_computation.3 | loop fusion | bytes 2097156 | tf_op jit(solution)/shard_map/dynamic_slice | solution.py:372
  3.1 3.0 %collective-permute-start.16 = (bf16[256,2048]{1,0:T(8,128)(2,1)}, bf16[256,2048]{1,0:T(8,128)(2,1)}, u32[]{:S(2)}, u32[]{:S(2)}) collective-permute-start(bf16[256,2048]{1,0:T(8,128)(2,1)} %dynamic-slice_bitcast_fusion), channel_id=1, source_target_pairs={{0,2},{2,0},{1,3},{3,1},{4,6},{6,4},{5,7},{7,5},{8,10},{10,8},{9,1... | collective-permute-start | bytes 3145736 | tf_op jit(solution)/shard_map/ppermute | solution.py:108
  6.7 3.9 %dispatch.1 = (s32[8,256]{1,0:T(8,128)}, bf16[48,4224]{1,0:T(8,128)(2,1)}, bf16[48,4224]{1,0:T(8,128)(2,1)}, bf16[48,4224]{1,0:T(8,128)(2,1)}, bf16[48,4224]{1,0:T(8,128)(2,1)}) custom-call(s32[2]{0:T(128)} %pad_add_fusion.1.place_ref, bf16[256,4096]{1,0:T(8,128)(2,1)} %x_ref.3, f32[1,4096]{1,0:T(1,128)} %bitcast.24, s32[2,256]{1,0:T(2,128)} %bitcast.27, ...), custom_call_target="tpu_custom_call" | custom-call | tf_op jit(solution)/shard_map/dispatch/pallas_call | solution.py:178
  10.7 1.6 %collective-permute-start.4 = (bf16[48,4224]{1,0:T(8,128)(2,1)}, bf16[48,4224]{1,0:T(8,128)(2,1)S(1)}, u32[]{:S(2)}, u32[]{:S(2)}) collective-permute-start(bf16[48,4224]{1,0:T(8,128)(2,1)} %get-tuple-element.13), channel_id=1, source_target_pairs={{0,8},{8,16},{16,24},{24,0},{1,9},{9,17},{17,25},{25,1},{2,10},{10... | collective-permute-start | bytes 1216520 | tf_op jit(solution)/shard_map/ppermute | solution.py:113
  12.2 2.3 %collective-permute-start.6 = (bf16[48,4224]{1,0:T(8,128)(2,1)}, bf16[48,4224]{1,0:T(8,128)(2,1)S(1)}, u32[]{:S(2)}, u32[]{:S(2)}) collective-permute-start(bf16[48,4224]{1,0:T(8,128)(2,1)} %get-tuple-element.14), channel_id=1, source_target_pairs={{0,24},{8,0},{16,8},{24,16},{1,25},{9,1},{17,9},{25,17},{2,26},{10... | collective-permute-start | bytes 1216520 | tf_op jit(solution)/shard_map/ppermute | solution.py:113
  16.0 9.0 %collective-permute-done.4.refs_2_.refs_14_ = bf16[48,4224]{1,0:T(8,128)(2,1)S(1)} collective-permute-done((bf16[48,4224]{1,0:T(8,128)(2,1)}, bf16[48,4224]{1,0:T(8,128)(2,1)S(1)}, u32[]{:S(2)}, u32[]{:S(2)}) %collective-permute-start.4) | collective-permute-done | bytes 405536 | tf_op jit(solution)/shard_map/ppermute | solution.py:113
  25.0 12.4 %collective-permute-start.20 = (bf16[48,4224]{1,0:T(8,128)(2,1)}, bf16[48,4224]{1,0:T(8,128)(2,1)S(1)}, u32[]{:S(2)}, u32[]{:S(2)}) collective-permute-start(bf16[48,4224]{1,0:T(8,128)(2,1)} %get-tuple-element.17), channel_id=1, source_target_pairs={{0,16},{8,24},{16,0},{24,8},{1,17},{9,25},{17,1},{25,9},{2,18},{10... | collective-permute-start | bytes 1216520 | tf_op jit(solution)/shard_map/ppermute | solution.py:113
  39.4 10.2 %collective-permute-done.20.refs_0_.refs_4_ = bf16[48,4224]{1,0:T(8,128)(2,1)S(1)} collective-permute-done((bf16[48,4224]{1,0:T(8,128)(2,1)}, bf16[48,4224]{1,0:T(8,128)(2,1)S(1)}, u32[]{:S(2)}, u32[]{:S(2)}) %collective-permute-start.20) | collective-permute-done | bytes 405536 | tf_op jit(solution)/shard_map/ppermute | solution.py:113
  52.6 2.1 %constant_dynamic-slice_fusion = (bf16[256,1024]{1,0:T(8,128)(2,1)S(1)}, bf16[256,1024]{1,0:T(8,128)(2,1)}) fusion(bf16[256,2048]{1,0:T(8,128)(2,1)} %collective-permute-done.16, s32[]{:T(128)S(6)} %select_n.19, s32[]{:T(128)S(6)} %select_n.17), kind=kLoop, calls=%fused_computation.14 | loop fusion | bytes 2097160 | tf_op jit(solution)/shard_map/dynamic_slice | solution.py:381
  54.7 1.6 %collective-permute-start.21 = (bf16[48,4224]{1,0:T(8,128)(2,1)S(1)}, bf16[48,4224]{1,0:T(8,128)(2,1)}, u32[]{:S(2)}, u32[]{:S(2)}) collective-permute-start(bf16[48,4224]{1,0:T(8,128)(2,1)S(1)} %collective-permute-done.20.refs_0_.refs_4_), channel_id=1, source_target_pairs={{0,4},{4,0},{1,5},{5,1},{2,6},{6,2},{3,7},{7,3},{8,12},{12,8},{9,1... | collective-permute-start | bytes 1216520 | tf_op jit(solution)/shard_map/ppermute | solution.py:108
  58.1 9.2 %expand.2.own_ref = bf16[576,256]{1,0:T(8,128)(2,1)} custom-call(s32[1]{0:T(128)} %bitcast.10.pair_ref, bf16[48,4224]{1,0:T(8,128)(2,1)} %get-tuple-element.12.refs_0_.refs_12_, bf16[48,4224]{1,0:T(8,128)(2,1)} %collective-permute-done.3.refs_1_.refs_13_, bf16[48,4224]{1,0:T(8,128)(2,1)} %copy-done.4, ...), custom_call_target="tpu_custom_call" | custom-call | tf_op jit(solution)/shard_map/expand/pallas_call | solution.py:218
  68.5 8.6 %collective-permute-done.14.beside_ref = bf16[576,256]{1,0:T(8,128)(2,1)S(1)} collective-permute-done((bf16[576,256]{1,0:T(8,128)(2,1)}, bf16[576,256]{1,0:T(8,128)(2,1)S(1)}, u32[]{:S(2)}, u32[]{:S(2)}) %collective-permute-start.14) | collective-permute-done | bytes 294944 | tf_op jit(solution)/shard_map/ppermute | solution.py:108
  77.0 1.9 %pad_maximum_fusion.1 = bf16[576,512]{1,0:T(8,128)(2,1)} fusion(bf16[576,256]{1,0:T(8,128)(2,1)S(1)} %collective-permute-done.14.beside_ref, bf16[576,256]{1,0:T(8,128)(2,1)} %expand.2.own_ref), kind=kLoop, calls=%fused_computation.4 | loop fusion | flops 1179648 | bytes 1179648 | tf_op jit(solution)/shard_map/concatenate | solution.py:395
  79.6 3.0 %collective-permute-start = (bf16[16,1024]{1,0:T(8,128)(2,1)}, bf16[16,1024]{1,0:T(8,128)(2,1)}, u32[]{:S(2)}, u32[]{:S(2)}) collective-permute-start(bf16[16,1024]{1,0:T(8,128)(2,1)} %slice.24), channel_id=1, source_target_pairs={{0,4},{4,8},{8,12},{12,16},{16,20},{20,24},{24,28},{1,5},{5,9},{9,... | collective-permute-start | bytes 98312 | tf_op jit(solution)/shard_map/ppermute | solution.py:19
  83.4 6.9 %expand.3.own_ref = bf16[192,256]{1,0:T(8,128)(2,1)} custom-call(s32[1]{0:T(128)} %bitcast.10.pair_ref, bf16[48,4224]{1,0:T(8,128)(2,1)} %copy-done.3, bf16[48,4224]{1,0:T(8,128)(2,1)} %collective-permute-done.21.refs_1_.refs_5_, bf16[48,4224]{1,0:T(8,128)(2,1)} %copy-done.7, bf16[48,4224]{1,0:T(8,128)(2,1)} %collective-permute-done.23.refs_3_.refs_7_, ...), custom_call_target="tpu_custom_call" | custom-call | tf_op jit(solution)/shard_map/expand/pallas_call | solution.py:218
  91.4 4.1 %collective-permute-done.24.beside_ref = bf16[192,256]{1,0:T(8,128)(2,1)S(1)} collective-permute-done((bf16[192,256]{1,0:T(8,128)(2,1)}, bf16[192,256]{1,0:T(8,128)(2,1)S(1)}, u32[]{:S(2)}, u32[]{:S(2)}) %collective-permute-start.24) | collective-permute-done | bytes 98336 | tf_op jit(solution)/shard_map/ppermute | solution.py:108
  96.6 4.3 %contract.2 = (bf16[288,1024]{1,0:T(8,128)(2,1)}, bf16[288,1024]{1,0:T(8,128)(2,1)}) custom-call(bf16[576,256]{1,0:T(8,128)(2,1)} %expand.2.own_ref, bf16[576,256]{1,0:T(8,128)(2,1)} %copy-done.8, bf16[576,512]{1,0:T(8,128)(2,1)} %collective-permute-done.15.across_ref, bf16[256,1024]{1,0:T(8,128)(2,1)} %get-tuple-element.21.wo_ref, ...), custom_call_target="tpu_custom_call" | custom-call | tf_op jit(solution)/shard_map/contract/pallas_call | solution.py:255
  100.9 3.3 %collective-permute-start.18 = (bf16[288,1024]{1,0:T(8,128)(2,1)}, bf16[288,1024]{1,0:T(8,128)(2,1)S(1)}, u32[]{:S(2)}, u32[]{:S(2)}) collective-permute-start(bf16[288,1024]{1,0:T(8,128)(2,1)} %get-tuple-element.16), channel_id=1, source_target_pairs={{0,4},{4,0},{1,5},{5,1},{2,6},{6,2},{3,7},{7,3},{8,12},{12,8},{9,1... | collective-permute-start | bytes 1769480 | tf_op jit(solution)/shard_map/ppermute | solution.py:108
  106.1 3.0 %contract.3 = (bf16[96,1024]{1,0:T(8,128)(2,1)}, bf16[96,1024]{1,0:T(8,128)(2,1)}) custom-call(bf16[192,256]{1,0:T(8,128)(2,1)} %expand.3.own_ref, bf16[192,256]{1,0:T(8,128)(2,1)} %copy-done.11, bf16[192,512]{1,0:T(8,128)(2,1)} %copy-done.13, bf16[256,1024]{1,0:T(8,128)(2,1)} %get-tuple-element.21.wo_ref, bf16[256,1024]{1,0:T(8,128)(2,1)} %get-tuple-element.23.wb_ref, ...), custom_call_target="tpu_custom_call" | custom-call | tf_op jit(solution)/shard_map/contract/pallas_call | solution.py:255
  110.0 12.6 %collective-permute-done.26 = bf16[96,1024]{1,0:T(8,128)(2,1)S(1)} collective-permute-done((bf16[96,1024]{1,0:T(8,128)(2,1)}, bf16[96,1024]{1,0:T(8,128)(2,1)S(1)}, u32[]{:S(2)}, u32[]{:S(2)}) %collective-permute-start.26) | collective-permute-done | bytes 196640 | tf_op jit(solution)/shard_map/ppermute | solution.py:108
  124.9 3.1 %collective-permute-start.19 = (bf16[96,1024]{1,0:T(8,128)(2,1)S(1)}, bf16[96,1024]{1,0:T(8,128)(2,1)S(1)}, u32[]{:S(2)}, u32[]{:S(2)}) collective-permute-start(bf16[96,1024]{1,0:T(8,128)(2,1)S(1)} %pad_maximum_fusion.3), channel_id=1, source_target_pairs={{0,24},{8,0},{16,8},{24,16},{1,25},{9,1},{17,9},{25,17},{2,26},{10... | collective-permute-start | bytes 589832 | tf_op jit(solution)/shard_map/ppermute | solution.py:113
  129.6 7.4 %pool.1 = bf16[1024,1024]{1,0:T(8,128)(2,1)} custom-call(s32[2]{0:T(128)} %pad_add_fusion.place_ref, bf16[1024,1024]{1,0:T(8,128)(2,1)} %prev_ref.1, bf16[1024,1024]{1,0:T(8,128)(2,1)} %prev_ref.1, bf16[16,1024]{1,0:T(8,128)(2,1)} %collective-permute-done.halo_ref, f32[1040,1]{1,0:T(8,128)} %broadcast_in_dim.4.sq_ref.psq_ref, ...), custom_call_target="tpu_custom_call" | custom-call | tf_op jit(solution)/shard_map/pool/pallas_call | solution.py:316
  137.6 2.2 %collective-permute-done.27.refs_2_ = bf16[96,1024]{1,0:T(8,128)(2,1)S(1)} collective-permute-done((bf16[96,1024]{1,0:T(8,128)(2,1)S(1)}, bf16[96,1024]{1,0:T(8,128)(2,1)S(1)}, u32[]{:S(2)}, u32[]{:S(2)}) %collective-permute-start.27) | collective-permute-done | bytes 196640 | tf_op jit(solution)/shard_map/ppermute | solution.py:113
  141.1 2.8 %restore.1 = bf16[256,1024]{1,0:T(8,128)(2,1)} custom-call(s32[8,256]{1,0:T(8,128)} %get-tuple-element.11.key_ref, bf16[96,1024]{1,0:T(8,128)(2,1)} %pad_maximum_fusion.2.refs_0_, bf16[96,1024]{1,0:T(8,128)(2,1)} %copy-done.15, bf16[96,1024]{1,0:T(8,128)(2,1)} %copy-done.12, bf16[96,1024]{1,0:T(8,128)(2,1)} %copy-done.14), custom_call_target="tpu_custom_call" | custom-call | tf_op jit(solution)/shard_map/restore/pallas_call | solution.py:283
  (94 shorter events, 22.1 us)
Async XLA Ops:
  3.1 48.1 %collective-permute-start.16 = (bf16[256,2048]{1,0:T(8,128)(2,1)}, bf16[256,2048]{1,0:T(8,128)(2,1)}, u32[]{:S(2)}, u32[]{:S(2)}) collective-permute-start(bf16[256,2048]{1,0:T(8,128)(2,1)} %dynamic-slice_bitcast_fusion), channel_id=1, source_target_pairs={{0,2},{2,0},{1,3},{3,1},{4,6},{6,4},{5,7},{7,5},{8,10},{10,8},{9,1... | collective-permute-start | bytes 3145736 | tf_op jit(solution)/shard_map/ppermute | solution.py:108
  10.7 14.3 %collective-permute-start.4 = (bf16[48,4224]{1,0:T(8,128)(2,1)}, bf16[48,4224]{1,0:T(8,128)(2,1)S(1)}, u32[]{:S(2)}, u32[]{:S(2)}) collective-permute-start(bf16[48,4224]{1,0:T(8,128)(2,1)} %get-tuple-element.13), channel_id=1, source_target_pairs={{0,8},{8,16},{16,24},{24,0},{1,9},{9,17},{17,25},{25,1},{2,10},{10... | collective-permute-start | bytes 1216520 | tf_op jit(solution)/shard_map/ppermute | solution.py:113
  12.2 25.1 %collective-permute-start.6 = (bf16[48,4224]{1,0:T(8,128)(2,1)}, bf16[48,4224]{1,0:T(8,128)(2,1)S(1)}, u32[]{:S(2)}, u32[]{:S(2)}) collective-permute-start(bf16[48,4224]{1,0:T(8,128)(2,1)} %get-tuple-element.14), channel_id=1, source_target_pairs={{0,24},{8,0},{16,8},{24,16},{1,25},{9,1},{17,9},{25,17},{2,26},{10... | collective-permute-start | bytes 1216520 | tf_op jit(solution)/shard_map/ppermute | solution.py:113
  14.5 24.4 %collective-permute-start.3 = (bf16[48,4224]{1,0:T(8,128)(2,1)}, bf16[48,4224]{1,0:T(8,128)(2,1)}, u32[]{:S(2)}, u32[]{:S(2)}) collective-permute-start(bf16[48,4224]{1,0:T(8,128)(2,1)} %get-tuple-element.12.refs_0_.refs_12_), channel_id=1, source_target_pairs={{0,4},{4,0},{1,5},{5,1},{2,6},{6,2},{3,7},{7,3},{8,12},{12,8},{9,1... | collective-permute-start | bytes 1216520 | tf_op jit(solution)/shard_map/ppermute | solution.py:108
  16.0 23.4 %collective-permute-start.8 = (bf16[48,4224]{1,0:T(8,128)(2,1)}, bf16[48,4224]{1,0:T(8,128)(2,1)}, u32[]{:S(2)}, u32[]{:S(2)}) collective-permute-start(bf16[48,4224]{1,0:T(8,128)(2,1)} %get-tuple-element.12.refs_0_.refs_12_), channel_id=1, source_target_pairs={{0,1},{1,0},{2,3},{3,2},{4,5},{5,4},{6,7},{7,6},{8,9},{9,8},{10,11... | collective-permute-start | bytes 1216520 | tf_op jit(solution)/shard_map/ppermute | solution.py:108
  25.0 24.7 %collective-permute-start.20 = (bf16[48,4224]{1,0:T(8,128)(2,1)}, bf16[48,4224]{1,0:T(8,128)(2,1)S(1)}, u32[]{:S(2)}, u32[]{:S(2)}) collective-permute-start(bf16[48,4224]{1,0:T(8,128)(2,1)} %get-tuple-element.17), channel_id=1, source_target_pairs={{0,16},{8,24},{16,0},{24,8},{1,17},{9,25},{17,1},{25,9},{2,18},{10... | collective-permute-start | bytes 1216520 | tf_op jit(solution)/shard_map/ppermute | solution.py:113
  37.4 12.3 %collective-permute-start.5 = (bf16[48,4224]{1,0:T(8,128)(2,1)S(1)}, bf16[48,4224]{1,0:T(8,128)(2,1)}, u32[]{:S(2)}, u32[]{:S(2)}) collective-permute-start(bf16[48,4224]{1,0:T(8,128)(2,1)S(1)} %collective-permute-done.4.refs_2_.refs_14_), channel_id=1, source_target_pairs={{0,4},{4,0},{1,5},{5,1},{2,6},{6,2},{3,7},{7,3},{8,12},{12,8},{9,1... | collective-permute-start | bytes 1216520 | tf_op jit(solution)/shard_map/ppermute | solution.py:108
  38.9 12.3 %collective-permute-start.7 = (bf16[48,4224]{1,0:T(8,128)(2,1)S(1)}, bf16[48,4224]{1,0:T(8,128)(2,1)}, u32[]{:S(2)}, u32[]{:S(2)}) collective-permute-start(bf16[48,4224]{1,0:T(8,128)(2,1)S(1)} %collective-permute-done.6.refs_4_.refs_16_), channel_id=1, source_target_pairs={{0,4},{4,0},{1,5},{5,1},{2,6},{6,2},{3,7},{7,3},{8,12},{12,8},{9,1... | collective-permute-start | bytes 1216520 | tf_op jit(solution)/shard_map/ppermute | solution.py:108
  39.4 15.3 %collective-permute-start.9 = (bf16[48,4224]{1,0:T(8,128)(2,1)}, bf16[48,4224]{1,0:T(8,128)(2,1)}, u32[]{:S(2)}, u32[]{:S(2)}) collective-permute-start(bf16[48,4224]{1,0:T(8,128)(2,1)} %collective-permute-done.3.refs_1_.refs_13_), channel_id=1, source_target_pairs={{0,1},{1,0},{2,3},{3,2},{4,5},{5,4},{6,7},{7,6},{8,9},{9,8},{10,11... | collective-permute-start | bytes 1216520 | tf_op jit(solution)/shard_map/ppermute | solution.py:108
  49.7 8.4 %collective-permute-start.12 = (bf16[48,4224]{1,0:T(8,128)(2,1)S(1)}, bf16[48,4224]{1,0:T(8,128)(2,1)}, u32[]{:S(2)}, u32[]{:S(2)}) collective-permute-start(bf16[48,4224]{1,0:T(8,128)(2,1)S(1)} %collective-permute-done.6.refs_4_.refs_16_), channel_id=1, source_target_pairs={{0,1},{1,0},{2,3},{3,2},{4,5},{5,4},{6,7},{7,6},{8,9},{9,8},{10,11... | collective-permute-start | bytes 1216520 | tf_op jit(solution)/shard_map/ppermute | solution.py:108
  54.7 13.5 %collective-permute-start.21 = (bf16[48,4224]{1,0:T(8,128)(2,1)S(1)}, bf16[48,4224]{1,0:T(8,128)(2,1)}, u32[]{:S(2)}, u32[]{:S(2)}) collective-permute-start(bf16[48,4224]{1,0:T(8,128)(2,1)S(1)} %collective-permute-done.20.refs_0_.refs_4_), channel_id=1, source_target_pairs={{0,4},{4,0},{1,5},{5,1},{2,6},{6,2},{3,7},{7,3},{8,12},{12,8},{9,1... | collective-permute-start | bytes 1216520 | tf_op jit(solution)/shard_map/ppermute | solution.py:108
  58.1 37.6 %collective-permute-start.17 = (bf16[512,1024]{1,0:T(8,128)(2,1)}, bf16[512,1024]{1,0:T(8,128)(2,1)S(1)}, u32[]{:S(2)}, u32[]{:S(2)}) collective-permute-start(bf16[512,1024]{1,0:T(8,128)(2,1)} %pad_maximum_fusion), channel_id=1, source_target_pairs={{0,1},{1,0},{2,3},{3,2},{4,5},{5,4},{6,7},{7,6},{8,9},{9,8},{10,11... | collective-permute-start | bytes 3145736 | tf_op jit(solution)/shard_map/ppermute | solution.py:108
  67.4 9.7 %collective-permute-start.14 = (bf16[576,256]{1,0:T(8,128)(2,1)}, bf16[576,256]{1,0:T(8,128)(2,1)S(1)}, u32[]{:S(2)}, u32[]{:S(2)}) collective-permute-start(bf16[576,256]{1,0:T(8,128)(2,1)} %expand.2.own_ref), channel_id=1, source_target_pairs={{0,2},{2,0},{1,3},{3,1},{4,6},{6,4},{5,7},{7,5},{8,10},{10,8},{9,1... | collective-permute-start | bytes 884744 | tf_op jit(solution)/shard_map/ppermute | solution.py:108
  68.0 14.6 %collective-permute-start.22 = (bf16[48,4224]{1,0:T(8,128)(2,1)S(1)}, bf16[48,4224]{1,0:T(8,128)(2,1)S(1)}, u32[]{:S(2)}, u32[]{:S(2)}) collective-permute-start(bf16[48,4224]{1,0:T(8,128)(2,1)S(1)} %collective-permute-done.20.refs_0_.refs_4_), channel_id=1, source_target_pairs={{0,1},{1,0},{2,3},{3,2},{4,5},{5,4},{6,7},{7,6},{8,9},{9,8},{10,11... | collective-permute-start | bytes 1216520 | tf_op jit(solution)/shard_map/ppermute | solution.py:108
  68.2 15.2 %collective-permute-start.23 = (bf16[48,4224]{1,0:T(8,128)(2,1)}, bf16[48,4224]{1,0:T(8,128)(2,1)}, u32[]{:S(2)}, u32[]{:S(2)}) collective-permute-start(bf16[48,4224]{1,0:T(8,128)(2,1)} %collective-permute-done.21.refs_1_.refs_5_), channel_id=1, source_target_pairs={{0,1},{1,0},{2,3},{3,2},{4,5},{5,4},{6,7},{7,6},{8,9},{9,8},{10,11... | collective-permute-start | bytes 1216520 | tf_op jit(solution)/shard_map/ppermute | solution.py:108
  79.0 16.7 %collective-permute-start.15 = (bf16[576,512]{1,0:T(8,128)(2,1)}, bf16[576,512]{1,0:T(8,128)(2,1)}, u32[]{:S(2)}, u32[]{:S(2)}) collective-permute-start(bf16[576,512]{1,0:T(8,128)(2,1)} %pad_maximum_fusion.1), channel_id=1, source_target_pairs={{0,1},{1,0},{2,3},{3,2},{4,5},{5,4},{6,7},{7,6},{8,9},{9,8},{10,11... | collective-permute-start | bytes 1769480 | tf_op jit(solution)/shard_map/ppermute | solution.py:108
  79.6 24.6 %collective-permute-start = (bf16[16,1024]{1,0:T(8,128)(2,1)}, bf16[16,1024]{1,0:T(8,128)(2,1)}, u32[]{:S(2)}, u32[]{:S(2)}) collective-permute-start(bf16[16,1024]{1,0:T(8,128)(2,1)} %slice.24), channel_id=1, source_target_pairs={{0,4},{4,8},{8,12},{12,16},{16,20},{20,24},{24,28},{1,5},{5,9},{9,... | collective-permute-start | bytes 98312 | tf_op jit(solution)/shard_map/ppermute | solution.py:19
  95.5 9.8 %collective-permute-start.25 = (bf16[192,512]{1,0:T(8,128)(2,1)S(1)}, bf16[192,512]{1,0:T(8,128)(2,1)S(1)}, u32[]{:S(2)}, u32[]{:S(2)}) collective-permute-start(bf16[192,512]{1,0:T(8,128)(2,1)S(1)} %pad_maximum_fusion.4), channel_id=1, source_target_pairs={{0,1},{1,0},{2,3},{3,2},{4,5},{5,4},{6,7},{7,6},{8,9},{9,8},{10,11... | collective-permute-start | bytes 589832 | tf_op jit(solution)/shard_map/ppermute | solution.py:108
  100.9 22.7 %collective-permute-start.18 = (bf16[288,1024]{1,0:T(8,128)(2,1)}, bf16[288,1024]{1,0:T(8,128)(2,1)S(1)}, u32[]{:S(2)}, u32[]{:S(2)}) collective-permute-start(bf16[288,1024]{1,0:T(8,128)(2,1)} %get-tuple-element.16), channel_id=1, source_target_pairs={{0,4},{4,0},{1,5},{5,1},{2,6},{6,2},{3,7},{7,3},{8,12},{12,8},{9,1... | collective-permute-start | bytes 1769480 | tf_op jit(solution)/shard_map/ppermute | solution.py:108
  109.1 13.6 %collective-permute-start.26 = (bf16[96,1024]{1,0:T(8,128)(2,1)}, bf16[96,1024]{1,0:T(8,128)(2,1)S(1)}, u32[]{:S(2)}, u32[]{:S(2)}) collective-permute-start(bf16[96,1024]{1,0:T(8,128)(2,1)} %get-tuple-element.19), channel_id=1, source_target_pairs={{0,4},{4,0},{1,5},{5,1},{2,6},{6,2},{3,7},{7,3},{8,12},{12,8},{9,1... | collective-permute-start | bytes 589832 | tf_op jit(solution)/shard_map/ppermute | solution.py:108
  109.4 19.1 %collective-permute-start.2 = (f32[1040]{0:T(1024)S(1)}, f32[1040]{0:T(1024)S(1)}, u32[]{:S(2)}, u32[]{:S(2)}) collective-permute-start(f32[1040]{0:T(1024)S(1)} %fusion), channel_id=1, source_target_pairs={{0,2},{2,0},{1,3},{3,1},{4,6},{6,4},{5,7},{7,5},{8,10},{10,8},{9,1... | collective-permute-start | bytes 12488 | tf_op jit(solution)/shard_map/ppermute | solution.py:108
  123.6 16.2 %collective-permute-start.27 = (bf16[96,1024]{1,0:T(8,128)(2,1)S(1)}, bf16[96,1024]{1,0:T(8,128)(2,1)S(1)}, u32[]{:S(2)}, u32[]{:S(2)}) collective-permute-start(bf16[96,1024]{1,0:T(8,128)(2,1)S(1)} %add_convert_fusion.1), channel_id=1, source_target_pairs={{0,16},{8,24},{16,0},{24,8},{1,17},{9,25},{17,1},{25,9},{2,18},{10... | collective-permute-start | bytes 589832 | tf_op jit(solution)/shard_map/ppermute | solution.py:113
  124.0 15.8 %collective-permute-start.28 = (bf16[96,1024]{1,0:T(8,128)(2,1)S(1)}, bf16[96,1024]{1,0:T(8,128)(2,1)S(1)}, u32[]{:S(2)}, u32[]{:S(2)}) collective-permute-start(bf16[96,1024]{1,0:T(8,128)(2,1)S(1)} %pad_maximum_fusion.5), channel_id=1, source_target_pairs={{0,8},{8,16},{16,24},{24,0},{1,9},{9,17},{17,25},{25,1},{2,10},{10... | collective-permute-start | bytes 589832 | tf_op jit(solution)/shard_map/ppermute | solution.py:113
  124.9 15.5 %collective-permute-start.19 = (bf16[96,1024]{1,0:T(8,128)(2,1)S(1)}, bf16[96,1024]{1,0:T(8,128)(2,1)S(1)}, u32[]{:S(2)}, u32[]{:S(2)}) collective-permute-start(bf16[96,1024]{1,0:T(8,128)(2,1)S(1)} %pad_maximum_fusion.3), channel_id=1, source_target_pairs={{0,24},{8,0},{16,8},{24,16},{1,25},{9,1},{17,9},{25,17},{2,26},{10... | collective-permute-start | bytes 589832 | tf_op jit(solution)/shard_map/ppermute | solution.py:113
  (21 other events, 207.7 us)
